TPU v7x, 32 devices: a whole 2x2x4 slice. The times are simulated.
32 devices in a mesh: sp: 8 (over z, x), dp: 4 (over y, core).
Axes of the slice: x: 2, y: 2, z: 4, core: 2. Of those that a mesh axis runs over, the one named last changes fastest.
Arguments:
- layer_activity: bfloat16 [4, 1024, 2048], P('dp', 'sp'), may hold values from -6 to 6
- writer_matrix: bfloat16 [2048, 256], P('dp'), may hold values from -0.125 to 0.125
- reader_matrix: bfloat16 [2048, 256], P('dp'), may hold values from -0.125 to 0.125
- source_unfiltered: bfloat16 [4, 1024, 2048], P('dp', 'sp'), may hold values from -6 to 6
- switch_raw_signal: bfloat16 [4, 1024, 2048], P('dp', 'sp'), may hold values from -6 to 6
- saved_result: bfloat16 [4, 1024, 2048], P('dp', 'sp'), may hold values from -6 to 6
- final_adjoint: bfloat16 [4, 1024, 2048], P('dp', 'sp'), may hold values from -6 to 6
- delta_raw: bfloat16 [4, 1024, 32], P('dp', 'sp'), may hold values from -4 to 4
- extra_logdrop: float32 [4, 1024, 32], P('dp', None, 'sp'), may hold values from 0 to 2.1
- source_filter_coefs: float32 [5, 2048], P(None, 'sp'), may hold values from -2.5 to 2.5
- writer_filter_coefs: float32 [5, 256], replicated, may hold values from -2.5 to 2.5
- reader_filter_coefs: float32 [5, 256], replicated, may hold values from -2.5 to 2.5
- delta_offset: float32 [32], P('sp'), may hold values from -7.5 to -6
- fading_exponents: float32 [32], P('sp'), may hold values from -6 to 3.4
- direct_factor: float32 [32], P('sp'), may hold values from 0.1 to 1.9
- rescale_factor: float32 [2048], replicated, may hold values from 0.1 to 1.9
Outputs:
- d_hidden: bfloat16 [4, 1024, 2048], P('dp', 'sp')
- d_x_raw: bfloat16 [4, 1024, 2048], P('dp', 'sp')
- d_gate: bfloat16 [4, 1024, 2048], P('dp', 'sp')
- d_dt_raw: bfloat16 [4, 1024, 32], P('dp', 'sp')
- d_w_b: float32 [2048, 256], P('dp')
- d_w_c: float32 [2048, 256], P('dp')
All inputs are finite; a program needn't handle non-finite values.
Results may differ from a plain program's by a relative error of at most 0.012.
Values may be sent and summed in bfloat16 or wider, within the bound.
A program may use at most 128 MiB of HBM per device.

v0:
```python
import jax
import jax.numpy as jnp
from jax import lax
from jax.sharding import PartitionSpec as P

HEADS = 32
HEAD_DIM = 64
STATE = 128
GROUPS = 2
NORM_GROUPS = 8
CONV_K = 5
BLOCK = 128
INNER = 2048
EPSILON = 1e-06
highest = lax.Precision.HIGHEST


def centred_conv(values, tap_weights):
    sample_window = values.shape[0]
    reach_side = (tap_weights.shape[0] - 1) // 2
    padded = jnp.pad(values, ((reach_side, reach_side), (0, 0)))
    summed = jnp.zeros_like(values)
    for offset in range(tap_weights.shape[0]):
        summed = summed + tap_weights[offset][None, :] * padded[offset : offset + sample_window]
    return summed


def one_channel_scan(
    source_unfiltered,
    writer_unfiltered,
    reader_unfiltered,
    delta_raw,
    extra_logdrop,
    source_filter_coefs,
    writer_filter_coefs,
    reader_filter_coefs,
    delta_offset,
    fading_exponents,
    direct_factor,
):
    inputs = jax.nn.silu(centred_conv(source_unfiltered, source_filter_coefs))
    keys_b = jax.nn.silu(centred_conv(writer_unfiltered, writer_filter_coefs))
    reads_c = jax.nn.silu(centred_conv(reader_unfiltered, reader_filter_coefs))
    smooth_delta = jax.nn.softplus(delta_raw + delta_offset)
    channel_fading = smooth_delta * jnp.exp(fading_exponents) + extra_logdrop
    cumulative = jnp.cumsum(channel_fading)
    sample_window = source_unfiltered.shape[0]
    blocks = sample_window // BLOCK
    driven = (inputs * smooth_delta[:, None]).reshape(blocks, BLOCK, -1)
    keyed = keys_b.reshape(blocks, BLOCK, -1)
    reading = reads_c.reshape(blocks, BLOCK, -1)
    levels = cumulative.reshape(blocks, BLOCK)
    within = jnp.exp(-jnp.abs(levels[:, :, None] - levels[:, None, :]))
    scores = jnp.einsum("ktn,ksn->kts", reading, keyed, precision=highest) * within
    output = jnp.einsum("kts,ksp->ktp", scores, driven, precision=highest)
    block_ends = levels[:, -1]
    block_starts = levels[:, 0]
    block_order = jnp.arange(blocks, dtype=jnp.int32)
    prev_end = jnp.concatenate([cumulative[:1], block_ends[:-1]])
    next_start = jnp.concatenate([block_starts[1:], cumulative[-1:]])
    weight_fwd = jnp.exp(levels - block_ends[:, None])
    state_fwd = jnp.einsum(
        "ksn,ksp->knp", keyed * weight_fwd[:, :, None], driven, precision=highest
    )
    mask_fwd = (block_order[None, :] < block_order[:, None]).astype(cumulative.dtype)
    link_fwd = jnp.exp(-jnp.abs(prev_end[:, None] - block_ends[None, :])) * mask_fwd
    carry_fwd = jnp.einsum("kj,jnp->knp", link_fwd, state_fwd, precision=highest)
    read_fwd = reading * jnp.exp(prev_end[:, None] - levels)[:, :, None]
    weight_bwd = jnp.exp(block_starts[:, None] - levels)
    state_bwd = jnp.einsum(
        "ksn,ksp->knp", keyed * weight_bwd[:, :, None], driven, precision=highest
    )
    mask_bwd = (block_order[None, :] > block_order[:, None]).astype(cumulative.dtype)
    link_bwd = jnp.exp(-jnp.abs(next_start[:, None] - block_starts[None, :])) * mask_bwd
    carry_bwd = jnp.einsum("kj,jnp->knp", link_bwd, state_bwd, precision=highest)
    read_bwd = reading * jnp.exp(levels - next_start[:, None])[:, :, None]
    output = output + jnp.einsum("ktn,knp->ktp", read_fwd, carry_fwd, precision=highest)
    output = output + jnp.einsum("ktn,knp->ktp", read_bwd, carry_bwd, precision=highest)
    return output.reshape(sample_window, -1) + direct_factor * inputs


def channelwise_derivs(
    source_unfiltered,
    writer_unfiltered,
    reader_unfiltered,
    delta_raw,
    extra_logdrop,
    source_filter_coefs,
    writer_filter_coefs,
    reader_filter_coefs,
    delta_offset,
    fading_exponents,
    direct_factor,
    result_adjoint,
):

    def forward(source_filtered, writer_filtered, reader_filtered, delta_argument):
        return one_channel_scan(
            source_filtered,
            writer_filtered,
            reader_filtered,
            delta_argument,
            extra_logdrop,
            source_filter_coefs,
            writer_filter_coefs,
            reader_filter_coefs,
            delta_offset,
            fading_exponents,
            direct_factor,
        )

    primal, pullback = jax.vjp(
        forward,
        source_unfiltered.astype(jnp.float32),
        writer_unfiltered.astype(jnp.float32),
        reader_unfiltered.astype(jnp.float32),
        delta_raw.astype(jnp.float32),
    )
    source_derivative, writer_derivative, reader_derivative, delta_derivative = pullback(
        result_adjoint.astype(jnp.float32)
    )
    return (
        source_derivative.astype(jnp.bfloat16),
        writer_derivative.astype(jnp.bfloat16),
        reader_derivative.astype(jnp.bfloat16),
        delta_derivative.astype(jnp.bfloat16),
    )


def gated_norm(values, gating, rescale_factor):
    mixed = values * jax.nn.silu(gating)
    grouped = mixed.reshape(mixed.shape[0], NORM_GROUPS, -1)
    scaled = grouped * lax.rsqrt(jnp.mean(grouped * grouped, axis=-1, keepdims=True) + EPSILON)
    return scaled.reshape(mixed.shape) * rescale_factor


def norm_backward(saved_result, switch_raw_signal, final_adjoint, rescale_factor):
    primal, pullback = jax.vjp(
        lambda values, gating: gated_norm(values, gating, rescale_factor),
        saved_result.astype(jnp.float32),
        switch_raw_signal.astype(jnp.float32),
    )
    d_values, d_gates = pullback(final_adjoint.astype(jnp.float32))
    return (d_values.astype(jnp.bfloat16), d_gates.astype(jnp.bfloat16))


def spread_heads(columns, tokens):
    grouped = columns.reshape(tokens, GROUPS, 1, STATE)
    copied = jnp.broadcast_to(grouped, (tokens, GROUPS, HEADS // GROUPS, STATE))
    return copied.reshape(1, tokens, HEADS * STATE)


def heads_first(values, window, local_channels, width):
    return jnp.transpose(values.reshape(window, local_channels, width), (1, 0, 2))


def local(
    layer_activity,
    writer_matrix,
    reader_matrix,
    source_unfiltered,
    switch_raw_signal,
    saved_result,
    final_adjoint,
    delta_raw,
    extra_logdrop,
    source_filter_coefs,
    writer_filter_coefs,
    reader_filter_coefs,
    delta_offset,
    fading_exponents,
    direct_factor,
    rescale_factor,
):
    tokens = layer_activity.shape[1]
    width_in = layer_activity.shape[2]
    latent_dimension = GROUPS * STATE
    data_devices = lax.axis_size("dp")
    local_channels = delta_offset.shape[0]
    per_group = HEADS // GROUPS
    weights = lax.all_gather(
        jnp.concatenate([writer_matrix, reader_matrix], axis=1), "dp", axis=0, tiled=True
    )
    token_rows = layer_activity.reshape(tokens, width_in)
    projected = jnp.dot(token_rows, weights, preferred_element_type=jnp.float32).astype(
        jnp.bfloat16
    )
    result_adjoint, d_gate = norm_backward(
        saved_result.reshape(tokens, INNER),
        switch_raw_signal.reshape(tokens, INNER),
        final_adjoint.reshape(tokens, INNER),
        rescale_factor,
    )
    copies_b = spread_heads(projected[:, :latent_dimension], tokens)
    copies_c = spread_heads(projected[:, latent_dimension:], tokens)
    heads_x, heads_b, heads_c, heads_dt, heads_dy = (
        lax.all_to_all(source_unfiltered, "sp", split_axis=2, concat_axis=1, tiled=True),
        lax.all_to_all(copies_b, "sp", split_axis=2, concat_axis=1, tiled=True),
        lax.all_to_all(copies_c, "sp", split_axis=2, concat_axis=1, tiled=True),
        lax.all_to_all(delta_raw, "sp", split_axis=2, concat_axis=1, tiled=True),
        lax.all_to_all(
            result_adjoint.reshape(1, tokens, INNER), "sp", split_axis=2, concat_axis=1, tiled=True
        ),
    )
    window = heads_x.shape[1]
    first_head = lax.axis_index("sp") * local_channels
    head_ids = first_head + jnp.arange(local_channels, dtype=jnp.int32)
    chooser = (
        head_ids[:, None] // per_group == jnp.arange(GROUPS, dtype=jnp.int32)[None, :]
    ).astype(jnp.float32)
    writer_filter_fn = jnp.einsum(
        "kgn,hg->hkn",
        writer_filter_coefs.reshape(CONV_K, GROUPS, STATE),
        chooser,
        precision=highest,
    )
    reader_filter_fn = jnp.einsum(
        "kgn,hg->hkn",
        reader_filter_coefs.reshape(CONV_K, GROUPS, STATE),
        chooser,
        precision=highest,
    )
    source_filter_fn = jnp.transpose(
        source_filter_coefs.reshape(CONV_K, local_channels, HEAD_DIM), (1, 0, 2)
    )
    per_head = jax.vmap(channelwise_derivs)
    source_derivative, writer_derivative, reader_derivative, delta_derivative = per_head(
        heads_first(heads_x, window, local_channels, HEAD_DIM),
        heads_first(heads_b, window, local_channels, STATE),
        heads_first(heads_c, window, local_channels, STATE),
        heads_dt.reshape(window, local_channels).T,
        extra_logdrop.reshape(window, local_channels).T,
        source_filter_fn,
        writer_filter_fn,
        reader_filter_fn,
        delta_offset,
        fading_exponents,
        direct_factor,
        heads_first(heads_dy, window, local_channels, HEAD_DIM),
    )
    back_x, back_b, back_c, back_dt = (
        lax.all_to_all(
            jnp.transpose(source_derivative, (1, 0, 2)).reshape(
                1, window, local_channels * HEAD_DIM
            ),
            "sp",
            split_axis=1,
            concat_axis=2,
            tiled=True,
        ),
        lax.all_to_all(
            jnp.transpose(writer_derivative, (1, 0, 2)).reshape(1, window, local_channels * STATE),
            "sp",
            split_axis=1,
            concat_axis=2,
            tiled=True,
        ),
        lax.all_to_all(
            jnp.transpose(reader_derivative, (1, 0, 2)).reshape(1, window, local_channels * STATE),
            "sp",
            split_axis=1,
            concat_axis=2,
            tiled=True,
        ),
        lax.all_to_all(
            delta_derivative.T.reshape(1, window, local_channels),
            "sp",
            split_axis=1,
            concat_axis=2,
            tiled=True,
        ),
    )
    summed_b = jnp.sum(back_b.reshape(tokens, GROUPS, per_group, STATE).astype(jnp.float32), axis=2)
    summed_c = jnp.sum(back_c.reshape(tokens, GROUPS, per_group, STATE).astype(jnp.float32), axis=2)
    gradients = jnp.concatenate(
        [
            summed_b.reshape(tokens, latent_dimension).astype(jnp.bfloat16),
            summed_c.reshape(tokens, latent_dimension).astype(jnp.bfloat16),
        ],
        axis=1,
    )
    d_hidden = jnp.einsum(
        "tc,dc->td", gradients, weights, preferred_element_type=jnp.float32
    ).astype(jnp.bfloat16)
    column_block = lax.all_to_all(layer_activity, "dp", split_axis=2, concat_axis=0, tiled=True)
    all_columns = column_block.reshape(data_devices * tokens, width_in // data_devices)
    all_grads = lax.all_gather(gradients, "dp", axis=0, tiled=True)
    local_rows = jnp.einsum("td,tc->dc", all_columns, all_grads, preferred_element_type=jnp.float32)
    total_grad = lax.psum(local_rows, "sp")
    return (
        d_hidden.reshape(1, tokens, width_in),
        back_x,
        d_gate.reshape(1, tokens, INNER),
        back_dt,
        total_grad[:, :latent_dimension],
        total_grad[:, latent_dimension:],
    )


def solution(mesh):
    in_specs = (
        P("dp", "sp", None),
        P("dp", None),
        P("dp", None),
        P("dp", "sp", None),
        P("dp", "sp", None),
        P("dp", "sp", None),
        P("dp", "sp", None),
        P("dp", "sp", None),
        P("dp", None, "sp"),
        P(None, "sp"),
        P(),
        P(),
        P("sp"),
        P("sp"),
        P("sp"),
        P(),
    )
    out_specs = (
        P("dp", "sp", None),
        P("dp", "sp", None),
        P("dp", "sp", None),
        P("dp", "sp", None),
        P("dp", None),
        P("dp", None),
    )
    return jax.shard_map(local, mesh=mesh, in_specs=in_specs, out_specs=out_specs, check_vma=False)
```

profile of v0, /device:TPU:0, one launch (start us, length us, event | category | flops | bytes accessed | tf_op | source)
XLA Modules:
  0.0 509.0 jit_solution(16484277088458486737)
XLA Ops:
  11.6 7.3 %all-to-all-start.1 = ((bf16[8,2,256]{2,1,0:T(2,128)(2,1)}), bf16[8,2,256]{2,1,0:T(2,128)(2,1)S(1)}, u32[]{:S(2)}, u32[]{:S(2)}) async-start(bf16[8,2,256]{2,1,0:T(2,128)(2,1)} %reshape.408), calls=%async_computation.1 | async-start | bytes 16384 | tf_op jit(solution)/shard_map/all_to_all | solution.py:200
  21.4 11.6 %reduce.19 = bf16[2048,128]{1,0:T(8,128)(2,1)S(1)} reduce(bf16[2048,1,128]{2,1,0:T(2,128)(2,1)S(1)} %bitcast.410, bf16[]{:T(256)} %broadcast.265), dimensions={1}, to_apply=%bitcast.316.reduce_sub_computation | reduce | bytes 1048578
  38.1 11.6 %reduce.14 = bf16[2048,128]{1,0:T(8,128)(2,1)S(1)} reduce(bf16[2048,1,128]{2,1,0:T(2,128)(2,1)S(1)} %bitcast.411, bf16[]{:T(256)} %broadcast.265), dimensions={1}, to_apply=%bitcast.304.reduce_sub_computation | reduce | bytes 1048578
  51.3 6.3 %all-to-all-start = ((bf16[8,2,16384]{2,1,0:T(2,128)(2,1)}), bf16[8,2,16384]{2,1,0:T(2,128)(2,1)}, u32[]{:S(2)}, u32[]{:S(2)}) async-start(bf16[8,2,16384]{2,1,0:T(2,128)(2,1)} %reshape.410), calls=%async_computation | async-start | bytes 1048576 | tf_op jit(solution)/shard_map/all_to_all | solution.py:197
  64.4 11.6 %reduce.13 = bf16[2048,128]{1,0:T(8,128)(2,1)S(1)} reduce(bf16[2048,1,128]{2,1,0:T(2,128)(2,1)S(1)} %bitcast.407, bf16[]{:T(256)} %broadcast.265), dimensions={1}, to_apply=%bitcast.306.reduce_sub_computation | reduce | bytes 1048578
  76.9 6.3 %all-to-all-start.3 = ((bf16[8,2,16384]{2,1,0:T(2,128)(2,1)}), bf16[8,2,16384]{2,1,0:T(2,128)(2,1)}, u32[]{:S(2)}, u32[]{:S(2)}) async-start(bf16[8,2,16384]{2,1,0:T(2,128)(2,1)} %reshape.412), calls=%async_computation.3 | async-start | bytes 1048576 | tf_op jit(solution)/shard_map/all_to_all | solution.py:201
  86.1 16.7 %copy.538 = bf16[1,128,4096]{1,0,2:T(2,128)(2,1)S(1)} copy(bf16[1,128,4096]{1,2,0:T(8,128)(2,1)S(1)} %bitcast.397) | data formatting | bytes 2097152 | tf_op jit(solution)/shard_map/reshape | solution.py:150
  102.8 22.4 %reduce.11 = bf16[4096,128]{1,0:T(8,128)(2,1)S(1)} reduce(bf16[4096,1,128]{2,1,0:T(2,128)(2,1)S(1)} %bitcast.391, bf16[]{:T(256)} %broadcast.265), dimensions={1}, to_apply=%bitcast.364.reduce_sub_computation | reduce | bytes 2097154
  126.4 6.5 %all-to-all-start.4 = ((bf16[8,2,32768]{2,1,0:T(2,128)(2,1)}), bf16[8,2,32768]{2,1,0:T(2,128)(2,1)S(1)}, u32[]{:S(2)}, u32[]{:S(2)}) async-start(bf16[8,2,32768]{2,1,0:T(2,128)(2,1)} %reshape.406), calls=%async_computation.4 | async-start | bytes 2097152 | tf_op jit(solution)/shard_map/all_to_all | solution.py:198
  135.3 16.7 %copy.539 = bf16[1,128,4096]{1,0,2:T(2,128)(2,1)S(1)} copy(bf16[1,128,4096]{1,2,0:T(8,128)(2,1)S(1)} %bitcast.398) | data formatting | bytes 2097152 | tf_op jit(solution)/shard_map/reshape | solution.py:150
  152.1 23.3 %reduce.10 = bf16[4096,128]{1,0:T(8,128)(2,1)} reduce(bf16[4096,1,128]{2,1,0:T(2,128)(2,1)S(1)} %bitcast.392, bf16[]{:T(256)} %broadcast.265), dimensions={1}, to_apply=%bitcast.365.reduce_sub_computation | reduce | bytes 2097154
  177.7 6.2 %all-to-all-start.2 = ((bf16[8,2,32768]{2,1,0:T(2,128)(2,1)}), bf16[8,2,32768]{2,1,0:T(2,128)(2,1)}, u32[]{:S(2)}, u32[]{:S(2)}) async-start(bf16[8,2,32768]{2,1,0:T(2,128)(2,1)} %reshape.404), calls=%async_computation.2 | async-start | bytes 2097152 | tf_op jit(solution)/shard_map/all_to_all | solution.py:199
  208.8 4.3 reshape.405
  217.7 4.4 fusion.40
  231.3 4.7 fusion.90
  236.0 4.4 fusion.35
  245.7 4.5 multiply_reduce_fusion.1
  265.1 6.4 %fusion.208 = (f32[4,8,128]{2,1,0:T(8,128)S(1)}, f32[4,8,128]{2,1,0:T(8,128)S(1)}, f32[4,8,128,128]{3,2,1,0:T(8,128)}) fusion(f32[4,8,128,128]{3,2,1,0:T(8,128)S(1)} %copy-done.5, f32[4,8,128,128]{3,2,1,0:T(8,128)S(1)} %bitcast.380, f32[4,8,128,128]{3,2,1,0:T(8,128)S(1)} %bitcast.374, f32[4,8,128]{2,1,0:T(8,128)S(1)} %broadcast_add_fusion), kind=kOutput, calls=%fused_computation.322 | convolution fusion | flops 812113920 | bytes 8437760 | tf_op jit(solution)/shard_map/vmap(jvp(ktn,ksn->kts))/dot_general | solution.py:54
  271.4 6.6 %add_add_fusion.1 = f32[4,8,128,128]{3,2,1,0:T(8,128)} fusion(f32[4,8,128,128]{3,2,1,0:T(8,128)S(1)} %copy-done.6, f32[4,8,128,128]{3,2,1,0:T(8,128)S(1)} %get-tuple-element.122, f32[4,8,128,128]{3,2,1,0:T(8,128)S(1)} %bitcast.381, f32[4,8,128,128]{3,2,1,0:T(8,128)S(1)} %copy-done.5, f32[4,8,128]{2,1,0:T(8,128)S(1)} %broadcast_add_fusion, ...), kind=kOutput, calls=%fused_computation.64 | convolution fusion | flops 809500672 | bytes 10534912 | tf_op jit(solution)/shard_map/vmap(transpose(jvp(ktn,ksn->kts)))/dot_general | solution.py:54
  295.9 6.0 %copy.372 = bf16[1,1024,512]{2,0,1:T(2,128)(2,1)} copy(bf16[1,1024,512]{1,2,0:T(8,128)(2,1)} %bitcast.413) | data formatting | bytes 2097152 | tf_op jit(solution)/shard_map/reshape | solution.py:259
  301.9 9.0 %reduce.15 = bf16[1024,512]{1,0:T(8,128)(2,1)} reduce(bf16[1024,1,512]{2,1,0:T(2,128)(2,1)} %bitcast.393, bf16[]{:T(256)} %broadcast.265), dimensions={1}, to_apply=%bitcast.308.reduce_sub_computation | reduce | bytes 2097154
  313.5 4.4 all-to-all-start.6
  321.1 5.0 reduce-window.16
  333.3 5.9 %copy.359 = bf16[1,1024,512]{2,0,1:T(2,128)(2,1)} copy(bf16[1,1024,512]{1,2,0:T(8,128)(2,1)} %bitcast.414) | data formatting | bytes 2097152 | tf_op jit(solution)/shard_map/reshape | solution.py:252
  339.3 9.0 %reduce.16 = bf16[1024,512]{1,0:T(8,128)(2,1)} reduce(bf16[1024,1,512]{2,1,0:T(2,128)(2,1)} %bitcast.394, bf16[]{:T(256)} %broadcast.265), dimensions={1}, to_apply=%bitcast.310.reduce_sub_computation | reduce | bytes 2097154
  355.2 6.0 %all-to-all-start.5 = ((bf16[8,2,32768]{2,1,0:T(2,128)(2,1)}), bf16[8,2,32768]{2,1,0:T(2,128)(2,1)}, u32[]{:S(2)}, u32[]{:S(2)}) async-start(bf16[8,2,32768]{2,1,0:T(2,128)(2,1)} %reshape.416), calls=%async_computation.5 | async-start | bytes 2097152 | tf_op jit(solution)/shard_map/all_to_all | solution.py:251
  361.3 5.5 %fusion.41 = f32[4,8,128,64]{2,3,1,0:T(8,128)S(1)} fusion(f32[4,8,128,128]{3,2,1,0:T(8,128)S(1)} %bitcast.376, f32[4,8,128]{2,1,0:T(8,128)S(1)} %get-tuple-element.102, f32[4,8,128,64]{2,1,3,0:T(8,128)} %copy-done.10), kind=kOutput, calls=%fused_computation.71 | convolution fusion | flops 403177472 | bytes 4210688 | tf_op jit(solution)/shard_map/vmap(transpose(jvp(ksn,ksp->knp)))/dot_general | solution.py:62
  388.8 6.0 %all-to-all-start.8 = ((bf16[8,2,256]{2,1,0:T(2,128)(2,1)}), bf16[8,2,256]{2,1,0:T(2,128)(2,1)S(1)}, u32[]{:S(2)}, u32[]{:S(2)}) async-start(bf16[8,2,256]{2,1,0:T(2,128)(2,1)} %reshape.420), calls=%async_computation.8 | async-start | bytes 16384 | tf_op jit(solution)/shard_map/all_to_all | solution.py:265
  400.9 7.3 %all_gather.7 = bf16[512,512]{0,1:T(8,128)(2,1)S(1)} all-gather(bf16[128,512]{0,1:T(8,128)(2,1)S(1)} %pad_maximum_fusion.1), channel_id=1, replica_groups=mesh['sp'=8,'dp'=4] {'dp'}, dimensions={0}, use_global_device_ids=true | all-gather | bytes 655360 | tf_op jit(solution)/shard_map/all_gather | solution.py:287
  408.3 6.0 %all-to-all-start.7 = ((bf16[8,2,16384]{2,1,0:T(2,128)(2,1)}), bf16[8,2,16384]{2,1,0:T(2,128)(2,1)S(1)}, u32[]{:S(2)}, u32[]{:S(2)}) async-start(bf16[8,2,16384]{2,1,0:T(2,128)(2,1)} %reshape.418), calls=%async_computation.7 | async-start | bytes 1048576 | tf_op jit(solution)/shard_map/all_to_all | solution.py:242
  417.4 17.0 %all-to-all-done.7 = bf16[8,2,16384]{2,1,0:T(2,128)(2,1)S(1)} async-done(((bf16[8,2,16384]{2,1,0:T(2,128)(2,1)}), bf16[8,2,16384]{2,1,0:T(2,128)(2,1)S(1)}, u32[]{:S(2)}, u32[]{:S(2)}) %all-to-all-start.7) | async-done | bytes 524320 | tf_op jit(solution)/shard_map/all_to_all | solution.py:242
  439.7 58.7 %all-reduce.26.cloned.1.call-done = f32[512,512]{0,1:T(8,128)} async-done(((f32[512,512]{0,1:T(8,128)}), f32[512,512]{0,1:T(8,128)}) %all-reduce.26.cloned.1.call-update) | async-done | bytes 1048592 | tf_op jit(solution)/shard_map/psum | solution.py:289
  (242 shorter events, 165.9 us)
Async XLA Ops:
  7.2 76.3 %all-gather.2.cloned.1.call-start = ((), (), s32[]{:S(2)}) async-start(), calls=%async_computation.10 | async-start | bytes 2621440 | tf_op jit(solution)/shard_map/all_gather | solution.py:181
  11.6 22.2 %all-to-all-start.1 = ((bf16[8,2,256]{2,1,0:T(2,128)(2,1)}), bf16[8,2,256]{2,1,0:T(2,128)(2,1)S(1)}, u32[]{:S(2)}, u32[]{:S(2)}) async-start(bf16[8,2,256]{2,1,0:T(2,128)(2,1)} %reshape.408), calls=%async_computation.1 | async-start | bytes 16384 | tf_op jit(solution)/shard_map/all_to_all | solution.py:200
  21.3 16.0 %copy-start.28 = (f32[2048]{0:T(1024)S(1)}, f32[2048]{0:T(1024)}, u32[]{:S(2)}) copy-start(f32[2048]{0:T(1024)} %param.31) | copy-start | bytes 24580
  21.3 16.0 %copy-start.27 = (bf16[1,128,2048]{2,1,0:T(8,128)(2,1)S(1)}, bf16[1,128,2048]{2,1,0:T(8,128)(2,1)}, u32[]{:S(2)}) copy-start(bf16[1,128,2048]{2,1,0:T(8,128)(2,1)} %param.19) | copy-start | bytes 1572868
  33.8 17.5 %all-to-all-start.9 = ((bf16[4,2,32768]{2,1,0:T(2,128)(2,1)}), bf16[4,2,32768]{2,1,0:T(2,128)(2,1)S(1)}, u32[]{:S(2)}, u32[]{:S(2)}) async-start(bf16[4,2,32768]{2,1,0:T(2,128)(2,1)} %reshape.422), calls=%async_computation.9 | async-start | bytes 1048576 | tf_op jit(solution)/shard_map/all_to_all | solution.py:285
  37.3 13.3 %copy-start.22 = (bf16[1,128,2048]{2,1,0:T(8,128)(2,1)S(1)}, bf16[1,128,2048]{2,1,0:T(8,128)(2,1)}, u32[]{:S(2)}) copy-start(bf16[1,128,2048]{2,1,0:T(8,128)(2,1)} %param.22) | copy-start | bytes 1572868
  38.1 12.6 %copy-start.21 = (bf16[1,128,2048]{2,1,0:T(8,128)(2,1)S(1)}, bf16[1,128,2048]{2,1,0:T(8,128)(2,1)}, u32[]{:S(2)}) copy-start(bf16[1,128,2048]{2,1,0:T(8,128)(2,1)} %param.21) | copy-start | bytes 1572868
  51.3 6.8 %copy-start.31 = (f32[5,256]{1,0:T(8,128)S(1)}, f32[5,256]{1,0:T(8,128)}, u32[]{:S(2)}) copy-start(f32[5,256]{1,0:T(8,128)} %param.26) | copy-start | bytes 15364
  51.3 7.0 %copy-start.23 = (bf16[4,2,32768]{2,1,0:T(2,128)(2,1)}, bf16[4,2,32768]{2,1,0:T(2,128)(2,1)S(1)}, u32[]{:S(2)}) copy-start(bf16[4,2,32768]{2,1,0:T(2,128)(2,1)S(1)} %all-to-all-done.9) | copy-start | bytes 1572868
  51.3 25.6 %all-to-all-start = ((bf16[8,2,16384]{2,1,0:T(2,128)(2,1)}), bf16[8,2,16384]{2,1,0:T(2,128)(2,1)}, u32[]{:S(2)}, u32[]{:S(2)}) async-start(bf16[8,2,16384]{2,1,0:T(2,128)(2,1)} %reshape.410), calls=%async_computation | async-start | bytes 1048576 | tf_op jit(solution)/shard_map/all_to_all | solution.py:197
  64.4 19.1 %copy-start.25 = (bf16[1,128,2048]{2,1,0:T(8,128)(2,1)S(1)}, bf16[1,128,2048]{2,1,0:T(8,128)(2,1)}, u32[]{:S(2)}) copy-start(bf16[1,128,2048]{2,1,0:T(8,128)(2,1)} %param.16) | copy-start | bytes 1572868
  76.9 49.5 %all-to-all-start.3 = ((bf16[8,2,16384]{2,1,0:T(2,128)(2,1)}), bf16[8,2,16384]{2,1,0:T(2,128)(2,1)}, u32[]{:S(2)}, u32[]{:S(2)}) async-start(bf16[8,2,16384]{2,1,0:T(2,128)(2,1)} %reshape.412), calls=%async_computation.3 | async-start | bytes 1048576 | tf_op jit(solution)/shard_map/all_to_all | solution.py:201
  125.2 7.7 %copy-start.35 = (f32[4]{0:T(128)S(1)}, f32[4]{0:T(128)}, u32[]{:S(2)}) copy-start(f32[4]{0:T(128)} %param.29) | copy-start | bytes 52
  125.2 7.7 %copy-start.32 = (f32[5,256]{1,0:T(8,128)S(1)}, f32[5,256]{1,0:T(8,128)}, u32[]{:S(2)}) copy-start(f32[5,256]{1,0:T(8,128)} %param.27) | copy-start | bytes 15364
  125.2 7.7 %copy-start.30 = (f32[5,256]{1,0:T(8,128)S(1)}, f32[5,256]{1,0:T(8,128)}, u32[]{:S(2)}) copy-start(f32[5,256]{1,0:T(8,128)} %param.25) | copy-start | bytes 15364
  125.3 8.1 %copy-start.29 = (f32[1,1024,4]{1,2,0:T(4,128)S(1)}, f32[1,1024,4]{1,2,0:T(4,128)}, u32[]{:S(2)}) copy-start(f32[1,1024,4]{1,2,0:T(4,128)} %param.24) | copy-start | bytes 49156
  125.3 8.1 %copy-start.33 = (f32[4]{0:T(128)S(1)}, f32[4]{0:T(128)}, u32[]{:S(2)}) copy-start(f32[4]{0:T(128)} %param.28) | copy-start | bytes 52
  126.4 51.2 %all-to-all-start.4 = ((bf16[8,2,32768]{2,1,0:T(2,128)(2,1)}), bf16[8,2,32768]{2,1,0:T(2,128)(2,1)S(1)}, u32[]{:S(2)}, u32[]{:S(2)}) async-start(bf16[8,2,32768]{2,1,0:T(2,128)(2,1)} %reshape.406), calls=%async_computation.4 | async-start | bytes 2097152 | tf_op jit(solution)/shard_map/all_to_all | solution.py:198
  175.4 9.0 %copy-start.24 = (bf16[4,2,32768]{2,1,0:T(2,128)(2,1)S(1)}, bf16[4,2,32768]{2,1,0:T(2,128)(2,1)}, u32[]{:S(2)}) copy-start(bf16[4,2,32768]{2,1,0:T(2,128)(2,1)} %copy-done.23) | copy-start | bytes 1572868
  177.7 7.4 %copy-start.15 = (bf16[8,2,32768]{2,1,0:T(2,128)(2,1)}, bf16[8,2,32768]{2,1,0:T(2,128)(2,1)S(1)}, u32[]{:S(2)}) copy-start(bf16[8,2,32768]{2,1,0:T(2,128)(2,1)S(1)} %all-to-all-done.4) | copy-start | bytes 3145732
  177.7 31.2 %all-to-all-start.2 = ((bf16[8,2,32768]{2,1,0:T(2,128)(2,1)}), bf16[8,2,32768]{2,1,0:T(2,128)(2,1)}, u32[]{:S(2)}, u32[]{:S(2)}) async-start(bf16[8,2,32768]{2,1,0:T(2,128)(2,1)} %reshape.404), calls=%async_computation.2 | async-start | bytes 2097152 | tf_op jit(solution)/shard_map/all_to_all | solution.py:199
  224.2 5.4 %copy-start = (f32[4,1024,128]{2,1,0:T(8,128)}, f32[4,1024,128]{2,1,0:T(8,128)S(1)}, u32[]{:S(2)}) copy-start(f32[4,1024,128]{2,1,0:T(8,128)S(1)} %copy.338) | copy-start | bytes 6291460
  260.0 5.0 copy-start.1
  271.4 6.6 %copy-start.4 = (bf16[1024,4,64]{0,2,1:T(8,128)(2,1)S(1)}, bf16[1024,4,64]{0,2,1:T(8,128)(2,1)}, u32[]{:S(2)}) copy-start(bf16[1024,4,64]{0,2,1:T(8,128)(2,1)} %copy-done.2) | copy-start | bytes 1572868
  313.5 41.7 %all-to-all-start.6 = ((bf16[8,2,32768]{2,1,0:T(2,128)(2,1)}), bf16[8,2,32768]{2,1,0:T(2,128)(2,1)}, u32[]{:S(2)}, u32[]{:S(2)}) async-start(bf16[8,2,32768]{2,1,0:T(2,128)(2,1)} %reshape.414), calls=%async_computation.6 | async-start | bytes 2097152 | tf_op jit(solution)/shard_map/all_to_all | solution.py:258
  355.2 33.5 %all-to-all-start.5 = ((bf16[8,2,32768]{2,1,0:T(2,128)(2,1)}), bf16[8,2,32768]{2,1,0:T(2,128)(2,1)}, u32[]{:S(2)}, u32[]{:S(2)}) async-start(bf16[8,2,32768]{2,1,0:T(2,128)(2,1)} %reshape.416), calls=%async_computation.5 | async-start | bytes 2097152 | tf_op jit(solution)/shard_map/all_to_all | solution.py:251
  361.3 5.5 %copy-start.12 = (f32[4,8,128,64]{2,1,3,0:T(8,128)S(1)}, f32[4,8,128,64]{2,1,3,0:T(8,128)}, u32[]{:S(2)}) copy-start(f32[4,8,128,64]{2,1,3,0:T(8,128)} %copy-done.11) | copy-start | bytes 3145732
  361.3 5.5 %copy-start.17 = (f32[4,8,128,64]{2,3,1,0:T(8,128)S(1)}, f32[4,8,128,64]{2,3,1,0:T(8,128)}, u32[]{:S(2)}) copy-start(f32[4,8,128,64]{2,3,1,0:T(8,128)} %fusion.26) | copy-start | bytes 3145732
  388.8 19.5 %all-to-all-start.8 = ((bf16[8,2,256]{2,1,0:T(2,128)(2,1)}), bf16[8,2,256]{2,1,0:T(2,128)(2,1)S(1)}, u32[]{:S(2)}, u32[]{:S(2)}) async-start(bf16[8,2,256]{2,1,0:T(2,128)(2,1)} %reshape.420), calls=%async_computation.8 | async-start | bytes 16384 | tf_op jit(solution)/shard_map/all_to_all | solution.py:265
  400.6 13.7 %copy-start.26 = (bf16[4,1,128,512]{3,2,0,1:T(8,128)(2,1)S(1)}, bf16[4,1,128,512]{3,2,0,1:T(8,128)(2,1)}, u32[]{:S(2)}) copy-start(bf16[4,1,128,512]{3,2,0,1:T(8,128)(2,1)} %copy.390) | copy-start | bytes 1572868
  408.3 26.1 %all-to-all-start.7 = ((bf16[8,2,16384]{2,1,0:T(2,128)(2,1)}), bf16[8,2,16384]{2,1,0:T(2,128)(2,1)S(1)}, u32[]{:S(2)}, u32[]{:S(2)}) async-start(bf16[8,2,16384]{2,1,0:T(2,128)(2,1)} %reshape.418), calls=%async_computation.7 | async-start | bytes 1048576 | tf_op jit(solution)/shard_map/all_to_all | solution.py:242
  414.3 84.2 %all-reduce.26.cloned.1.call-start = ((), (), s32[]{:S(2)}) async-start(), calls=%async_computation.11 | async-start | bytes 2097152 | tf_op jit(solution)/shard_map/psum | solution.py:289
  (16 other events, 54.7 us)
Sparse Core Ops, SparseCore 0:
  10.1 25.2 all-gather.1
  418.6 79.7 all-reduce.25
where the time goes:
time: 519 us; the launch traced here: 509 us
  other arithmetic  148 us (29%)
  local copies, waits for them, and re-layouts  125 us (24%)
  waiting for transfers between devices  78.6 us (15%)
  matrix products  76 us (15%)
  starting transfers between devices  58.5 us (11%)
  between operations  15.7 us (3%)
  blocking collectives  7.34 us (1%)
    unnamed x15, other arithmetic  108 us
    psum x1, waiting for transfers between devices, local(): total_grad = lax.psum(local_rows, 'sp')  58.7 us
    unnamed x111, local copies, waits for them, and re-layouts  46.7 us
    reshape x2, local copies, waits for them, and re-layouts, spread_heads(): return copied.reshape(1, tokens, HEADS * STATE)  33.5 us
    dot_general x3, matrix products, one_channel_scan(): jnp.einsum('ktn,ksn->kts', reading, keyed, precision=highest) * within  17.2 us
    all_to_all x1, waiting for transfers between devices, local(): lax.all_to_all(jnp.transpose(source_derivative, (1, 0, 2)).reshape(1, win...  17 us
    another operation x8, other arithmetic  14.2 us
    dot_general x3, matrix products, one_channel_scan(): jnp.einsum('ksn,ksp->knp', keyed * weight_fwd[:, :, None], driven, precis...  12.4 us
  transfers between devices with their start and end apart: 12, of which 3 were waited for; matrix products, arithmetic and copies ran while one was open for 47% of the time, Pallas kernels for 0%

commit v1 on v0

--- a/solution.py
+++ b/solution.py
@@ -286,7 +286,8 @@
     all_columns = column_block.reshape(data_devices * tokens, width_in // data_devices)
     all_grads = lax.all_gather(gradients, "dp", axis=0, tiled=True)
     local_rows = jnp.einsum("td,tc->dc", all_columns, all_grads, preferred_element_type=jnp.float32)
-    total_grad = lax.psum(local_rows, "sp")
+    parts = lax.all_gather(local_rows, "sp", axis=0, tiled=False)
+    total_grad = parts.sum(axis=0)
     return (
         d_hidden.reshape(1, tokens, width_in),
         back_x,

time: 519 us -> 558 us (1.075)
  local copies, waits for them, and re-layouts: 125 us -> 153 us
  other arithmetic: 148 us -> 155 us
    psum x1 -> x0, waiting for transfers between devices: 58.7 us -> none  [local(): total_grad = lax.psum(local_rows, 'sp')]
    all_gather x0 -> x1, waiting for transfers between devices: none -> 39.4 us  [local(): parts = lax.all_gather(local_rows, 'sp', axis=0, tiled=False)]
    unnamed x111 -> x108, local copies, waits for them, and re-layouts: 46.7 us -> 72.5 us
    all_to_all x1, waiting for transfers between devices: 17 us -> 29.2 us  [local(): lax.all_to_all(jnp.transpose(source_derivative, (1, 0, 2)).reshape(1, win...]
    all_to_all x1, waiting for transfers between devices: 0.01 us -> 9.42 us  [local(): lax.all_to_all(jnp.transpose(writer_derivative, (1, 0, 2)).reshape(1, win...]
  transfers between devices with their start and end apart: 12 -> 12, of which waited for: 3 -> 4; matrix products, arithmetic and copies ran while one was open for 47% -> 64% of each run, Pallas kernels for 0% -> 0%
where the time goes in v1:
time: 558 us; the launch traced here: 550 us
  other arithmetic  155 us (28%)
  local copies, waits for them, and re-layouts  153 us (27%)
  waiting for transfers between devices  81.5 us (15%)
  matrix products  79.7 us (14%)
  starting transfers between devices  58 us (10%)
  between operations  15.4 us (3%)
  blocking collectives  7.8 us (1%)
    unnamed x15, other arithmetic  109 us
    unnamed x108, local copies, waits for them, and re-layouts  72.5 us
    all_gather x1, waiting for transfers between devices, local(): parts = lax.all_gather(local_rows, 'sp', axis=0, tiled=False)  39.4 us
    reshape x2, local copies, waits for them, and re-layouts, spread_heads(): return copied.reshape(1, tokens, HEADS * STATE)  33.5 us
    all_to_all x1, waiting for transfers between devices, local(): lax.all_to_all(jnp.transpose(source_derivative, (1, 0, 2)).reshape(1, win...  29.2 us
    dot_general x3, matrix products, one_channel_scan(): jnp.einsum('ktn,ksn->kts', reading, keyed, precision=highest) * within  21.2 us
    another operation x8, other arithmetic  14.3 us
    dot_general x3, matrix products, one_channel_scan(): jnp.einsum('ksn,ksp->knp', keyed * weight_bwd[:, :, None], driven, precis...  11.2 us
  transfers between devices with their start and end apart: 12, of which 4 were waited for; matrix products, arithmetic and copies ran while one was open for 64% of the time, Pallas kernels for 0%

profile of v1, /device:TPU:0, one launch (start us, length us, event | category | flops | bytes accessed | tf_op | source)
XLA Modules:
  0.0 550.4 jit_solution(6040868372961339566)
XLA Ops:
  11.8 7.3 %all-to-all-start.1 = ((bf16[8,2,256]{2,1,0:T(2,128)(2,1)}), bf16[8,2,256]{2,1,0:T(2,128)(2,1)S(1)}, u32[]{:S(2)}, u32[]{:S(2)}) async-start(bf16[8,2,256]{2,1,0:T(2,128)(2,1)} %reshape.409), calls=%async_computation.1 | async-start | bytes 16384 | tf_op jit(solution)/shard_map/all_to_all | solution.py:200
  23.9 12.3 %reduce.14 = bf16[2048,128]{1,0:T(8,128)(2,1)} reduce(bf16[2048,1,128]{2,1,0:T(2,128)(2,1)S(1)} %bitcast.417, bf16[]{:T(256)} %broadcast.265), dimensions={1}, to_apply=%bitcast.309.reduce_sub_computation | reduce | bytes 1048578
  38.2 6.6 %all-to-all-start = ((bf16[8,2,16384]{2,1,0:T(2,128)(2,1)}), bf16[8,2,16384]{2,1,0:T(2,128)(2,1)}, u32[]{:S(2)}, u32[]{:S(2)}) async-start(bf16[8,2,16384]{2,1,0:T(2,128)(2,1)} %reshape.411), calls=%async_computation | async-start | bytes 1048576 | tf_op jit(solution)/shard_map/all_to_all | solution.py:197
  51.8 11.6 %reduce.13 = bf16[2048,128]{1,0:T(8,128)(2,1)S(1)} reduce(bf16[2048,1,128]{2,1,0:T(2,128)(2,1)S(1)} %bitcast.414, bf16[]{:T(256)} %broadcast.265), dimensions={1}, to_apply=%bitcast.311.reduce_sub_computation | reduce | bytes 1048578
  64.4 6.2 %all-to-all-start.3 = ((bf16[8,2,16384]{2,1,0:T(2,128)(2,1)}), bf16[8,2,16384]{2,1,0:T(2,128)(2,1)}, u32[]{:S(2)}, u32[]{:S(2)}) async-start(bf16[8,2,16384]{2,1,0:T(2,128)(2,1)} %reshape.413), calls=%async_computation.3 | async-start | bytes 1048576 | tf_op jit(solution)/shard_map/all_to_all | solution.py:201
  73.5 16.7 %copy.533 = bf16[1,128,4096]{1,0,2:T(2,128)(2,1)S(1)} copy(bf16[1,128,4096]{1,2,0:T(8,128)(2,1)S(1)} %bitcast.403) | data formatting | bytes 2097152 | tf_op jit(solution)/shard_map/reshape | solution.py:150
  90.2 22.4 %reduce.11 = bf16[4096,128]{1,0:T(8,128)(2,1)S(1)} reduce(bf16[4096,1,128]{2,1,0:T(2,128)(2,1)S(1)} %bitcast.397, bf16[]{:T(256)} %broadcast.265), dimensions={1}, to_apply=%bitcast.369.reduce_sub_computation | reduce | bytes 2097154
  113.8 6.4 %all-to-all-start.4 = ((bf16[8,2,32768]{2,1,0:T(2,128)(2,1)}), bf16[8,2,32768]{2,1,0:T(2,128)(2,1)S(1)}, u32[]{:S(2)}, u32[]{:S(2)}) async-start(bf16[8,2,32768]{2,1,0:T(2,128)(2,1)} %reshape.407), calls=%async_computation.4 | async-start | bytes 2097152 | tf_op jit(solution)/shard_map/all_to_all | solution.py:198
  121.1 11.5 %reduce.19 = bf16[2048,128]{1,0:T(8,128)(2,1)S(1)} reduce(bf16[2048,1,128]{2,1,0:T(2,128)(2,1)S(1)} %bitcast.412, bf16[]{:T(256)} %broadcast.265), dimensions={1}, to_apply=%bitcast.321.reduce_sub_computation | reduce | bytes 1048578
  135.8 16.7 %copy.534 = bf16[1,128,4096]{1,0,2:T(2,128)(2,1)S(1)} copy(bf16[1,128,4096]{1,2,0:T(8,128)(2,1)S(1)} %bitcast.404) | data formatting | bytes 2097152 | tf_op jit(solution)/shard_map/reshape | solution.py:150
  152.6 23.4 %reduce.10 = bf16[4096,128]{1,0:T(8,128)(2,1)} reduce(bf16[4096,1,128]{2,1,0:T(2,128)(2,1)S(1)} %bitcast.398, bf16[]{:T(256)} %broadcast.265), dimensions={1}, to_apply=%bitcast.370.reduce_sub_computation | reduce | bytes 2097154
  178.2 6.5 %all-to-all-start.2 = ((bf16[8,2,32768]{2,1,0:T(2,128)(2,1)}), bf16[8,2,32768]{2,1,0:T(2,128)(2,1)}, u32[]{:S(2)}, u32[]{:S(2)}) async-start(bf16[8,2,32768]{2,1,0:T(2,128)(2,1)} %reshape.405), calls=%async_computation.2 | async-start | bytes 2097152 | tf_op jit(solution)/shard_map/all_to_all | solution.py:199
  235.0 4.7 fusion.90
  239.7 4.5 fusion.35
  249.3 4.8 multiply_reduce_fusion.1
  280.0 6.1 %copy.366 = bf16[1,1024,512]{2,0,1:T(2,128)(2,1)} copy(bf16[1,1024,512]{1,2,0:T(8,128)(2,1)} %bitcast.419) | data formatting | bytes 2097152 | tf_op jit(solution)/shard_map/reshape | solution.py:259
  286.1 9.0 %reduce.15 = bf16[1024,512]{1,0:T(8,128)(2,1)} reduce(bf16[1024,1,512]{2,1,0:T(2,128)(2,1)} %bitcast.399, bf16[]{:T(256)} %broadcast.265), dimensions={1}, to_apply=%bitcast.313.reduce_sub_computation | reduce | bytes 2097154
  302.2 8.4 %add_add_fusion.1 = f32[4,8,128,128]{3,2,1,0:T(8,128)} fusion(f32[4,8,128,128]{3,2,1,0:T(8,128)} %fusion.90, f32[4,8,128,128]{3,2,1,0:T(8,128)} %get-tuple-element.110, f32[4,8,128,128]{3,2,1,0:T(8,128)} %bitcast.385, f32[4,8,128,128]{3,2,1,0:T(8,128)} %fusion.88, f32[4,8,128]{2,1,0:T(8,128)S(1)} %broadcast_add_fusion, ...), kind=kOutput, calls=%fused_computation.65 | convolution fusion | flops 809500672 | bytes 10534912 | tf_op jit(solution)/shard_map/vmap(transpose(jvp(ktn,ksn->kts)))/dot_general | solution.py:54
  320.4 6.2 %copy.353 = bf16[1,1024,512]{2,0,1:T(2,128)(2,1)} copy(bf16[1,1024,512]{1,2,0:T(8,128)(2,1)} %bitcast.420) | data formatting | bytes 2097152 | tf_op jit(solution)/shard_map/reshape | solution.py:252
  326.6 9.1 %reduce.16 = bf16[1024,512]{1,0:T(8,128)(2,1)} reduce(bf16[1024,1,512]{2,1,0:T(2,128)(2,1)} %bitcast.400, bf16[]{:T(256)} %broadcast.265), dimensions={1}, to_apply=%bitcast.315.reduce_sub_computation | reduce | bytes 2097154
  338.3 6.0 %all-to-all-start.5 = ((bf16[8,2,32768]{2,1,0:T(2,128)(2,1)}), bf16[8,2,32768]{2,1,0:T(2,128)(2,1)}, u32[]{:S(2)}, u32[]{:S(2)}) async-start(bf16[8,2,32768]{2,1,0:T(2,128)(2,1)} %reshape.417), calls=%async_computation.5 | async-start | bytes 2097152 | tf_op jit(solution)/shard_map/all_to_all | solution.py:251
  350.1 5.8 %reshape.416 = bf16[1024,1,512]{2,1,0:T(2,128)(2,1)} reshape(bf16[8,2,32768]{2,1,0:T(2,128)(2,1)} %all-to-all-done.6) | data formatting | bytes 2097152
  361.1 9.4 %all-to-all-done.5 = bf16[8,2,32768]{2,1,0:T(2,128)(2,1)} async-done(((bf16[8,2,32768]{2,1,0:T(2,128)(2,1)}), bf16[8,2,32768]{2,1,0:T(2,128)(2,1)}, u32[]{:S(2)}, u32[]{:S(2)}) %all-to-all-start.5) | async-done | bytes 1048608 | tf_op jit(solution)/shard_map/all_to_all | solution.py:251
  370.5 5.8 %reshape.418 = bf16[1024,1,512]{2,1,0:T(2,128)(2,1)} reshape(bf16[8,2,32768]{2,1,0:T(2,128)(2,1)} %all-to-all-done.5) | data formatting | bytes 2097152
  384.3 7.8 %all_gather.13 = bf16[512,512]{0,1:T(8,128)(2,1)S(1)} all-gather(bf16[128,512]{0,1:T(8,128)(2,1)S(1)} %pad_maximum_fusion.1), channel_id=1, replica_groups=mesh['sp'=8,'dp'=4] {'dp'}, dimensions={0}, use_global_device_ids=true | all-gather | bytes 655360 | tf_op jit(solution)/shard_map/all_gather | solution.py:287
  393.6 5.1 fusion.209
  402.8 8.5 %fusion.208 = (f32[4,8,128]{2,1,0:T(8,128)S(1)}, f32[4,8,128]{2,1,0:T(8,128)S(1)}, f32[4,8,128,128]{3,2,1,0:T(8,128)}) fusion(f32[4,8,128,128]{3,2,1,0:T(8,128)} %fusion.88, f32[4,8,128,128]{3,2,1,0:T(8,128)} %bitcast.386, f32[4,8,128,128]{3,2,1,0:T(8,128)S(1)} %bitcast.380, f32[4,8,128]{2,1,0:T(8,128)S(1)} %broadcast_add_fusion), kind=kOutput, calls=%fused_computation.323 | convolution fusion | flops 812113920 | bytes 8437760 | tf_op jit(solution)/shard_map/vmap(jvp(ktn,ksn->kts))/dot_general | solution.py:54
  411.4 5.1 reduce-window.16
  444.4 6.0 %all-to-all-start.7 = ((bf16[8,2,16384]{2,1,0:T(2,128)(2,1)}), bf16[8,2,16384]{2,1,0:T(2,128)(2,1)S(1)}, u32[]{:S(2)}, u32[]{:S(2)}) async-start(bf16[8,2,16384]{2,1,0:T(2,128)(2,1)} %reshape.419), calls=%async_computation.7 | async-start | bytes 1048576 | tf_op jit(solution)/shard_map/all_to_all | solution.py:242
  452.0 29.2 %all-to-all-done.7 = bf16[8,2,16384]{2,1,0:T(2,128)(2,1)S(1)} async-done(((bf16[8,2,16384]{2,1,0:T(2,128)(2,1)}), bf16[8,2,16384]{2,1,0:T(2,128)(2,1)S(1)}, u32[]{:S(2)}, u32[]{:S(2)}) %all-to-all-start.7) | async-done | bytes 524320 | tf_op jit(solution)/shard_map/all_to_all | solution.py:242
  486.7 39.4 %all-gather.6.cloned.1.call-done = f32[4096,512]{0,1:T(8,128)} async-done(((f32[512,512]{0,1:T(8,128)}), f32[4096,512]{0,1:T(8,128)}) %all-gather.6.cloned.1.call-update) | async-done | bytes 8388624 | tf_op jit(solution)/shard_map/all_gather | solution.py:289
  526.0 11.5 %copy.416 = f32[64,8,8,512]{3,2,1,0:T(8,128)S(1)} copy(f32[64,8,8,512]{3,1,2,0:T(8,128)} %bitcast.396) | data formatting | bytes 16777216
  (240 shorter events, 195.0 us)
Async XLA Ops:
  7.2 13.8 %copy-start.22 = (bf16[1,128,2048]{2,1,0:T(8,128)(2,1)S(1)}, bf16[1,128,2048]{2,1,0:T(8,128)(2,1)}, u32[]{:S(2)}) copy-start(bf16[1,128,2048]{2,1,0:T(8,128)(2,1)} %param.21) | copy-start | bytes 1572868
  7.2 63.7 %all-gather.4.cloned.1.call-start = ((), (), s32[]{:S(2)}) async-start(), calls=%async_computation.10 | async-start | bytes 2621440 | tf_op jit(solution)/shard_map/all_gather | solution.py:181
  9.1 11.9 %copy-start.21 = (bf16[1,128,2048]{2,1,0:T(8,128)(2,1)S(1)}, bf16[1,128,2048]{2,1,0:T(8,128)(2,1)}, u32[]{:S(2)}) copy-start(bf16[1,128,2048]{2,1,0:T(8,128)(2,1)} %param.20) | copy-start | bytes 1572868
  11.8 26.4 %all-to-all-start.1 = ((bf16[8,2,256]{2,1,0:T(2,128)(2,1)}), bf16[8,2,256]{2,1,0:T(2,128)(2,1)S(1)}, u32[]{:S(2)}, u32[]{:S(2)}) async-start(bf16[8,2,256]{2,1,0:T(2,128)(2,1)} %reshape.409), calls=%async_computation.1 | async-start | bytes 16384 | tf_op jit(solution)/shard_map/all_to_all | solution.py:200
  36.2 9.0 %copy-start.29 = (f32[5,256]{1,0:T(8,128)S(1)}, f32[5,256]{1,0:T(8,128)}, u32[]{:S(2)}) copy-start(f32[5,256]{1,0:T(8,128)} %param.26) | copy-start | bytes 15364
  38.2 26.2 %all-to-all-start = ((bf16[8,2,16384]{2,1,0:T(2,128)(2,1)}), bf16[8,2,16384]{2,1,0:T(2,128)(2,1)}, u32[]{:S(2)}, u32[]{:S(2)}) async-start(bf16[8,2,16384]{2,1,0:T(2,128)(2,1)} %reshape.411), calls=%async_computation | async-start | bytes 1048576 | tf_op jit(solution)/shard_map/all_to_all | solution.py:197
  51.8 19.0 %copy-start.23 = (bf16[1,128,2048]{2,1,0:T(8,128)(2,1)S(1)}, bf16[1,128,2048]{2,1,0:T(8,128)(2,1)}, u32[]{:S(2)}) copy-start(bf16[1,128,2048]{2,1,0:T(8,128)(2,1)} %param.16) | copy-start | bytes 1572868
  64.4 49.4 %all-to-all-start.3 = ((bf16[8,2,16384]{2,1,0:T(2,128)(2,1)}), bf16[8,2,16384]{2,1,0:T(2,128)(2,1)}, u32[]{:S(2)}, u32[]{:S(2)}) async-start(bf16[8,2,16384]{2,1,0:T(2,128)(2,1)} %reshape.413), calls=%async_computation.3 | async-start | bytes 1048576 | tf_op jit(solution)/shard_map/all_to_all | solution.py:201
  112.6 7.6 %copy-start.24 = (bf16[1,128,2048]{2,1,0:T(8,128)(2,1)S(1)}, bf16[1,128,2048]{2,1,0:T(8,128)(2,1)}, u32[]{:S(2)}) copy-start(bf16[1,128,2048]{2,1,0:T(8,128)(2,1)} %param.16) | copy-start | bytes 1572868
  113.8 7.2 %copy-start.33 = (f32[4]{0:T(128)S(1)}, f32[4]{0:T(128)}, u32[]{:S(2)}) copy-start(f32[4]{0:T(128)} %param.29) | copy-start | bytes 52
  113.8 7.2 %copy-start.30 = (f32[5,256]{1,0:T(8,128)S(1)}, f32[5,256]{1,0:T(8,128)}, u32[]{:S(2)}) copy-start(f32[5,256]{1,0:T(8,128)} %param.27) | copy-start | bytes 15364
  113.8 7.3 %copy-start.28 = (f32[5,256]{1,0:T(8,128)S(1)}, f32[5,256]{1,0:T(8,128)}, u32[]{:S(2)}) copy-start(f32[5,256]{1,0:T(8,128)} %param.25) | copy-start | bytes 15364
  113.8 64.4 %all-to-all-start.4 = ((bf16[8,2,32768]{2,1,0:T(2,128)(2,1)}), bf16[8,2,32768]{2,1,0:T(2,128)(2,1)S(1)}, u32[]{:S(2)}, u32[]{:S(2)}) async-start(bf16[8,2,32768]{2,1,0:T(2,128)(2,1)} %reshape.407), calls=%async_computation.4 | async-start | bytes 2097152 | tf_op jit(solution)/shard_map/all_to_all | solution.py:198
  120.2 13.6 %copy-start.27 = (f32[1,1024,4]{1,2,0:T(4,128)S(1)}, f32[1,1024,4]{1,2,0:T(4,128)}, u32[]{:S(2)}) copy-start(f32[1,1024,4]{1,2,0:T(4,128)} %param.24) | copy-start | bytes 49156
  120.2 13.6 %copy-start.31 = (f32[4]{0:T(128)S(1)}, f32[4]{0:T(128)}, u32[]{:S(2)}) copy-start(f32[4]{0:T(128)} %param.28) | copy-start | bytes 52
  178.2 10.3 %copy-start.18 = (bf16[8,2,32768]{2,1,0:T(2,128)(2,1)}, bf16[8,2,32768]{2,1,0:T(2,128)(2,1)S(1)}, u32[]{:S(2)}) copy-start(bf16[8,2,32768]{2,1,0:T(2,128)(2,1)S(1)} %all-to-all-done.4) | copy-start | bytes 3145732
  178.2 30.3 %all-to-all-start.2 = ((bf16[8,2,32768]{2,1,0:T(2,128)(2,1)}), bf16[8,2,32768]{2,1,0:T(2,128)(2,1)}, u32[]{:S(2)}, u32[]{:S(2)}) async-start(bf16[8,2,32768]{2,1,0:T(2,128)(2,1)} %reshape.405), calls=%async_computation.2 | async-start | bytes 2097152 | tf_op jit(solution)/shard_map/all_to_all | solution.py:199
  192.2 4.8 copy-start.2
  208.4 89.3 %all-to-all-start.9 = ((bf16[4,2,32768]{2,1,0:T(2,128)(2,1)}), bf16[4,2,32768]{2,1,0:T(2,128)(2,1)}, u32[]{:S(2)}, u32[]{:S(2)}) async-start(bf16[4,2,32768]{2,1,0:T(2,128)(2,1)} %reshape.423), calls=%async_computation.9 | async-start | bytes 1048576 | tf_op jit(solution)/shard_map/all_to_all | solution.py:285
  227.9 5.4 copy-start
  235.0 4.8 copy-start.12
  235.0 4.8 copy-start.16
  249.3 4.8 copy-start.14
  297.7 40.6 %all-to-all-start.6 = ((bf16[8,2,32768]{2,1,0:T(2,128)(2,1)}), bf16[8,2,32768]{2,1,0:T(2,128)(2,1)}, u32[]{:S(2)}, u32[]{:S(2)}) async-start(bf16[8,2,32768]{2,1,0:T(2,128)(2,1)} %reshape.415), calls=%async_computation.6 | async-start | bytes 2097152 | tf_op jit(solution)/shard_map/all_to_all | solution.py:258
  338.3 32.2 %all-to-all-start.5 = ((bf16[8,2,32768]{2,1,0:T(2,128)(2,1)}), bf16[8,2,32768]{2,1,0:T(2,128)(2,1)}, u32[]{:S(2)}, u32[]{:S(2)}) async-start(bf16[8,2,32768]{2,1,0:T(2,128)(2,1)} %reshape.417), calls=%async_computation.5 | async-start | bytes 2097152 | tf_op jit(solution)/shard_map/all_to_all | solution.py:251
  344.3 181.7 %all-gather.6.cloned.1.call-start = ((), (), s32[]{:S(2)}) async-start(), calls=%async_computation.11 | async-start | bytes 9437184 | tf_op jit(solution)/shard_map/all_gather | solution.py:289
  381.4 10.6 %copy-start.25 = (bf16[4,1,128,512]{3,2,0,1:T(8,128)(2,1)S(1)}, bf16[4,1,128,512]{3,2,0,1:T(8,128)(2,1)}, u32[]{:S(2)}) copy-start(bf16[4,1,128,512]{3,2,0,1:T(8,128)(2,1)} %copy.384) | copy-start | bytes 1572868
  393.5 5.4 copy-start.8
  393.5 5.4 copy-start.10
  424.2 4.2 copy-start.20
  433.0 11.4 %all-to-all-start.8 = ((bf16[8,2,256]{2,1,0:T(2,128)(2,1)}), bf16[8,2,256]{2,1,0:T(2,128)(2,1)S(1)}, u32[]{:S(2)}, u32[]{:S(2)}) async-start(bf16[8,2,256]{2,1,0:T(2,128)(2,1)} %reshape.421), calls=%async_computation.8 | async-start | bytes 16384 | tf_op jit(solution)/shard_map/all_to_all | solution.py:265
  444.4 36.9 %all-to-all-start.7 = ((bf16[8,2,16384]{2,1,0:T(2,128)(2,1)}), bf16[8,2,16384]{2,1,0:T(2,128)(2,1)S(1)}, u32[]{:S(2)}, u32[]{:S(2)}) async-start(bf16[8,2,16384]{2,1,0:T(2,128)(2,1)} %reshape.419), calls=%async_computation.7 | async-start | bytes 1048576 | tf_op jit(solution)/shard_map/all_to_all | solution.py:242
  (14 other events, 36.9 us)
Sparse Core Ops, SparseCore 0:
  10.1 25.2 all-gather.3
  393.6 132.3 all-gather.5
